TPU v7x, 32 devices: a whole 2x2x4 slice. The times are simulated.
32 devices in a mesh: ep: 4 (over y, x), tp: 8 (over z, core).
Axes of the slice: x: 2, y: 2, z: 4, core: 2. Of those that a mesh axis runs over, the one named last changes fastest.
Arguments:
- mixer_input: bfloat16 [6144, 1024], P(('ep', 'tp')), may hold values from -6 to 6
- mixer_gain: float32 [1024], replicated, may hold values from 0.1 to 1.9
- group_weight: bfloat16 [4, 256, 256], replicated, may hold values from -0.375 to 0.375
- mixer_scale: float32 [1024], replicated, may hold values from 0.1 to 1.9
- expert_input: bfloat16 [6144, 1024], P(('ep', 'tp')), may hold values from -6 to 6
- expert_gain: float32 [1024], replicated, may hold values from 0.1 to 1.9
- routes: int32 [6144, 2], P(('ep', 'tp')), may hold values from 0 to 3, all different within a row; in each aligned block of 192 rows (0 to 191, 192 to 383, ...) at most 144 rows name the same one
- route_weight: float32 [6144, 2], P(('ep', 'tp')), may hold values from 0.2 to 1
- w_gate: bfloat16 [4, 1024, 4096], P('ep', None, 'tp'), may hold values from -0.1875 to 0.1875
- w_up: bfloat16 [4, 1024, 4096], P('ep', None, 'tp'), may hold values from -0.1875 to 0.1875
- w_down: bfloat16 [4, 4096, 1024], P('ep', 'tp'), may hold values from -0.09375 to 0.09375
Outputs:
- mixer_out: bfloat16 [6144, 1024], P(('ep', 'tp'))
- expert_out: bfloat16 [6144, 1024], P(('ep', 'tp'))
Inputs may be any that keep to these rules, and one draw needn't show every extreme that they name: `routes`: each row names 2 different experts. Among the rows of one device no expert is named by more than 144 rows, and in some device's rows some expert is named exactly 144 times.
All inputs are finite; a program needn't handle non-finite values.
Results may differ from a plain program's by a relative error of at most 0.0076.
Values may be sent and summed in bfloat16 or wider, within the bound.
A program may use at most 128 MiB of HBM per device.

v0:
```python
import jax
import jax.numpy as jnp
from jax import lax
from jax.sharding import PartitionSpec as P

epsilon = 1e-06


def padded_2(value, sides, width):
    for axis, dim in sides:
        size, length = (lax.axis_size(axis), value.shape[dim])
        up = [(i, (i + 1) % size) for i in range(size - 1)]
        down = [(j, i) for i, j in up]
        last = lax.slice_in_dim(value, length - width, length, axis=dim)
        leading = lax.slice_in_dim(value, 0, width, axis=dim)
        before = lax.ppermute(last, axis, up)
        after = lax.ppermute(leading, axis, down)
        value = jnp.concatenate([before, value, after], axis=dim)
    return value


def normalize(row_values, gain):
    values = row_values.astype(jnp.float32)
    scaled = values * lax.rsqrt(jnp.mean(values * values, axis=-1, keepdims=True) + epsilon)
    return (scaled * gain).astype(jnp.bfloat16)


def pool_groups(padded, start_row, row_count, seq_length):
    group_width = padded.shape[1] // 4
    position = start_row + jnp.arange(row_count, dtype=jnp.int32)
    centre = padded[8 : 8 + row_count]
    pooled_parts = []
    for group_index in range(4):
        window = 2 ** (group_index + 1)
        reach_left = window // 2
        reach_right = window - 1 - reach_left
        group_cols = padded[:, group_index * group_width : (group_index + 1) * group_width]
        window_sum = group_cols[8 - reach_left : 8 - reach_left + row_count]
        for offset in range(1 - reach_left, reach_right + 1):
            window_sum = window_sum + group_cols[8 + offset : 8 + offset + row_count]
        cover = (
            jnp.minimum(position + reach_right + 1, seq_length)
            - jnp.maximum(position - reach_left, 0)
        ).astype(jnp.float32)
        pooled_parts.append(
            window_sum / cover[:, None]
            - centre[:, group_index * group_width : (group_index + 1) * group_width]
        )
    return jnp.stack(pooled_parts, axis=1).astype(jnp.bfloat16)


def on_device(
    mixer_input,
    mixer_gain,
    group_weight,
    mixer_scale,
    expert_input,
    expert_gain,
    routes,
    route_weight,
    w_gate,
    w_up,
    w_down,
):
    row_count = mixer_input.shape[0]
    normed = normalize(mixer_input, mixer_gain)
    padded = padded_2(normed, ((("ep", "tp"), 0),), 8)
    start_row = lax.axis_index(("ep", "tp")) * row_count
    seq_length = row_count * lax.axis_size(("ep", "tp"))
    pooled = pool_groups(padded.astype(jnp.float32), start_row, row_count, seq_length)
    mixed_groups = jnp.einsum(
        "tgi,gio->tgo", pooled, group_weight, preferred_element_type=jnp.float32
    )
    mixer_out = (mixed_groups.reshape(row_count, -1) * mixer_scale).astype(jnp.bfloat16)
    row_count = expert_input.shape[0]
    top_count = routes.shape[1]
    experts = lax.axis_size("ep") * w_gate.shape[0]
    capacity = 3 * top_count * row_count // (2 * experts)
    normed = normalize(expert_input, expert_gain)
    flat_route = routes.reshape(-1)
    onehot = (flat_route[:, None] == jnp.arange(experts, dtype=jnp.int32)[None, :]).astype(
        jnp.int32
    )
    before = jnp.cumsum(onehot, axis=0) - onehot
    slot_index = flat_route * capacity + jnp.sum(before * onehot, axis=1)
    places = (
        slot_index.reshape(row_count, top_count)[None, :, :]
        == jnp.arange(experts * capacity, dtype=jnp.int32)[:, None, None]
    )
    dispatch = jnp.any(places, axis=2).astype(jnp.bfloat16)
    outgoing = jnp.dot(dispatch, normed, preferred_element_type=jnp.float32).astype(jnp.bfloat16)
    arrived = lax.all_to_all(outgoing, "ep", split_axis=0, concat_axis=0, tiled=True)
    down_w = w_down[0]
    paired = jnp.stack((w_gate[0], w_up[0]), axis=0)
    portion = lax.all_gather(paired, "tp", axis=2, tiled=True)
    gate_part = jnp.dot(arrived, portion[0], preferred_element_type=jnp.float32)
    up_part = jnp.dot(arrived, portion[1], preferred_element_type=jnp.float32)
    hidden = (jax.nn.silu(gate_part) * up_part).astype(jnp.bfloat16)
    block_width = down_w.shape[0]
    portion = lax.all_gather(down_w, "tp", axis=0, tiled=True)
    blocks = portion.shape[0] // block_width
    hidden_part = hidden
    hidden_part = hidden_part.reshape(hidden_part.shape[0], blocks, block_width)
    block_terms = jnp.einsum(
        "rkf,kfd->krd",
        hidden_part,
        portion.reshape(blocks, block_width, portion.shape[1]),
        preferred_element_type=jnp.float32,
    )
    rounded = lax.optimization_barrier(block_terms.astype(jnp.bfloat16)).astype(jnp.float32)
    result = jnp.sum(rounded, axis=0)
    returned = lax.all_to_all(
        result.astype(jnp.bfloat16), "ep", split_axis=0, concat_axis=0, tiled=True
    )
    picked = (
        jnp.take(returned, slot_index, axis=0).astype(jnp.float32).reshape(row_count, top_count, -1)
    )
    expert_out = jnp.sum(picked * route_weight[:, :, None], axis=1).astype(jnp.bfloat16)
    return (mixer_out, expert_out)


def solution(mesh):
    placed = (
        P(("ep", "tp"), None),
        P(),
        P(),
        P(),
        P(("ep", "tp"), None),
        P(),
        P(("ep", "tp"), None),
        P(("ep", "tp"), None),
        P("ep", None, "tp"),
        P("ep", None, "tp"),
        P("ep", "tp", None),
    )
    return jax.shard_map(
        on_device,
        mesh=mesh,
        in_specs=placed,
        out_specs=(P(("ep", "tp"), None), P(("ep", "tp"), None)),
        check_vma=False,
    )
```

profile of v0, /device:TPU:0, one launch (start us, length us, event | category | flops | bytes accessed | tf_op | source)
XLA Modules:
  0.0 297.9 jit_solution(8162747445675623130)
XLA Ops:
  7.2 0.0 copy-start
  7.2 0.0 all-gather.4.cloned.1.call-start
  7.3 3.2 %pad_maximum_fusion = bf16[2,1024,512]{2,1,0:T(8,128)(2,1)} fusion(bf16[1,1024,512]{2,1,0:T(8,128)(2,1)} %param.20, bf16[1,1024,512]{2,1,0:T(8,128)(2,1)} %param.19), kind=kLoop, calls=%fused_computation.9 | loop fusion | flops 1048576 | bytes 4194304 | tf_op jit(solution)/shard_map/stack | solution.py:94
  10.5 0.0 all-gather.4.cloned.1.call-update
  10.5 0.0 all-gather.6.cloned.1.call-start
  10.5 0.7 all-gather.6.cloned.1.call-update
  11.2 0.8 copy.31
  12.0 0.1 eq.39
  12.2 0.1 reshape.140
  12.3 1.2 reduce-window.6
  13.6 0.2 slice_reduce_fusion
  13.8 0.2 reduce-window.9
  14.0 0.1 add_bitcast_fusion
  14.1 0.2 reduce_sum.54
  14.2 0.1 copy.33
  14.3 0.7 compare_and_fusion
  15.0 0.2 fusion.4
  15.2 1.2 fusion.8
  16.3 1.6 convolution_convert_fusion.1
  18.0 5.2 %all-to-all-start = ((bf16[4,144,1024]{2,1,0:T(8,128)(2,1)}), bf16[4,144,1024]{2,1,0:T(8,128)(2,1)S(1)}, u32[]{:S(2)}, u32[]{:S(2)}) async-start(bf16[4,144,1024]{2,1,0:T(8,128)(2,1)} %bitcast.6), calls=%async_computation | async-start | bytes 2359296 | tf_op jit(solution)/shard_map/all_to_all | solution.py:92
  23.2 0.2 fusion.5
  23.3 0.2 fusion.7
  23.5 1.5 collective-permute-start
  25.0 1.5 collective-permute-start.1
  26.5 0.1 copy.36
  26.6 0.1 mul.110
  26.8 0.2 copy.34
  27.0 0.1 copy.37
  27.1 2.6 collective-permute-done.1
  29.7 0.1 maximum_convert_fusion
  29.8 8.6 %all-to-all-done = bf16[4,144,1024]{2,1,0:T(8,128)(2,1)S(1)} async-done(((bf16[4,144,1024]{2,1,0:T(8,128)(2,1)}), bf16[4,144,1024]{2,1,0:T(8,128)(2,1)S(1)}, u32[]{:S(2)}, u32[]{:S(2)}) %all-to-all-start) | async-done | bytes 1179680 | tf_op jit(solution)/shard_map/all_to_all | solution.py:92
  38.4 126.4 %all-gather.4.cloned.1.call-done = bf16[2,1024,4096]{2,1,0:T(8,128)(2,1)} async-done(((bf16[2,1024,512]{2,1,0:T(8,128)(2,1)}), bf16[2,1024,4096]{2,1,0:T(8,128)(2,1)}) %all-gather.4.cloned.1.call-update) | async-done | bytes 16777232 | tf_op jit(solution)/shard_map/all_gather | solution.py:95
  164.8 11.0 %fusion = f32[576,4096]{1,0:T(8,128)} fusion(bf16[576,1024]{1,0:T(8,128)(2,1)S(1)} %bitcast.56, bf16[2,1024,4096]{2,1,0:T(8,128)(2,1)} %all-gather.4.cloned.1.call-done), kind=kOutput, calls=%fused_computation.3 | convolution fusion | flops 4831838208 | bytes 19005440 | tf_op jit(solution)/shard_map/dot_general | solution.py:97
  175.8 0.7 copy-done.8
  176.5 10.2 %multiply_convert_fusion = bf16[576,4096]{1,0:T(8,128)(2,1)} fusion(f32[576,4096]{1,0:T(8,128)} %fusion, bf16[576,1024]{1,0:T(8,128)(2,1)S(1)} %bitcast.57, bf16[2,1024,4096]{2,1,0:T(8,128)(2,1)S(1)} %copy-done.8), kind=kOutput, calls=%fused_computation.1 | convolution fusion | flops 4845993984 | bytes 23724032 | tf_op jit(solution)/shard_map/dot_general | solution.py:96
  186.6 59.9 %all-gather.6.cloned.1.call-done = bf16[1,4096,1024]{2,1,0:T(8,128)(2,1)} async-done(((bf16[1,512,1024]{2,1,0:T(8,128)(2,1)}), bf16[1,4096,1024]{2,1,0:T(8,128)(2,1)}) %all-gather.6.cloned.1.call-update) | async-done | bytes 8388624 | tf_op jit(solution)/shard_map/all_gather | solution.py:100
  246.5 11.5 %convolution_convert_fusion = bf16[8,576,1024]{2,1,0:T(8,128)(2,1)} fusion(bf16[8,512,1024]{2,1,0:T(8,128)(2,1)} %bitcast.59, bf16[72,8,8,512]{3,2,1,0:T(8,128)(2,1)} %bitcast.60), kind=kOutput, calls=%fused_computation.6 | convolution fusion | flops 4836556800 | bytes 22544384 | tf_op jit(solution)/shard_map/rkf,kfd->krd/dot_general | solution.py:104
  258.0 7.3 %reduce_sum.56 = bf16[576,1024]{1,0:T(8,128)(2,1)} reduce(bf16[8,576,1024]{2,1,0:T(8,128)(2,1)} %convolution_convert_fusion, bf16[]{:T(256)} %constant.71.clone.1), dimensions={0}, to_apply=%region_6.7 | reduce | flops 4128768 | bytes 10616834 | tf_op jit(solution)/shard_map/reduce_sum | solution.py:111
  265.3 3.9 %all-to-all-start.1 = ((bf16[4,144,1024]{2,1,0:T(8,128)(2,1)}), bf16[4,144,1024]{2,1,0:T(8,128)(2,1)S(1)}, u32[]{:S(2)}, u32[]{:S(2)}) async-start(bf16[4,144,1024]{2,1,0:T(8,128)(2,1)} %bitcast.54), calls=%async_computation.1 | async-start | bytes 2359296 | tf_op jit(solution)/shard_map/all_to_all | solution.py:112
  269.2 0.2 fusion.39
  269.5 0.3 fusion.36
  269.8 0.3 convolution_bitcast_fusion
  270.0 0.1 copy.39
  270.1 0.8 multiply_convert_fusion.1
  270.9 13.7 %all-to-all-done.1 = bf16[4,144,1024]{2,1,0:T(8,128)(2,1)S(1)} async-done(((bf16[4,144,1024]{2,1,0:T(8,128)(2,1)}), bf16[4,144,1024]{2,1,0:T(8,128)(2,1)S(1)}, u32[]{:S(2)}, u32[]{:S(2)}) %all-to-all-start.1) | async-done | bytes 1179680 | tf_op jit(solution)/shard_map/all_to_all | solution.py:112
  284.7 2.1 gather_fusion
  286.8 0.3 gather.7
  287.1 3.9 %multiply_reduce_fusion = bf16[192,1024]{1,0:T(8,128)(2,1)} fusion(bf16[192,2,1024]{2,1,0:T(2,128)(2,1)S(1)} %gather.7, pred[192,2]{1,0:T(8,128)(4,1)S(1)} %copy.34, f32[192,2]{1,0:T(8,128)S(1)} %copy.37), kind=kLoop, calls=%fused_computation.10 | loop fusion | flops 1376256 | bytes 1181568 | tf_op jit(solution)/shard_map/reduce_sum | solution.py:118
  (27 shorter events, 0.1 us)
Async XLA Ops:
  7.2 262.6 %copy-start = (bf16[4,256,256]{2,1,0:T(8,128)(2,1)S(1)}, bf16[4,256,256]{2,1,0:T(8,128)(2,1)}, u32[]{:S(2)}) copy-start(bf16[4,256,256]{2,1,0:T(8,128)(2,1)} %param.13) | copy-start | bytes 1572868
  7.2 19.3 %copy-start.3 = (s32[192,2]{0,1:T(2,128)S(1)}, s32[192,2]{0,1:T(2,128)}, u32[]{:S(2)}) copy-start(s32[192,2]{0,1:T(2,128)} %param.17) | copy-start | bytes 4612
  7.2 9.1 %copy-start.2 = (bf16[192,1024]{1,0:T(8,128)(2,1)S(1)}, bf16[192,1024]{1,0:T(8,128)(2,1)}, u32[]{:S(2)}) copy-start(bf16[192,1024]{1,0:T(8,128)(2,1)} %param.15) | copy-start | bytes 1179652
  7.2 9.1 %copy-start.4 = (f32[1024]{0:T(1024)S(1)}, f32[1024]{0:T(1024)}, u32[]{:S(2)}) copy-start(f32[1024]{0:T(1024)} %param.16) | copy-start | bytes 12292
  7.2 15.9 %copy-start.1 = (bf16[192,1024]{1,0:T(8,128)(2,1)S(1)}, bf16[192,1024]{1,0:T(8,128)(2,1)}, u32[]{:S(2)}) copy-start(bf16[192,1024]{1,0:T(8,128)(2,1)} %param.11) | copy-start | bytes 1179652
  7.2 16.1 %copy-start.5 = (f32[1024]{0:T(1024)S(1)}, f32[1024]{0:T(1024)}, u32[]{:S(2)}) copy-start(f32[1024]{0:T(1024)} %param.12) | copy-start | bytes 12292
  7.2 19.8 %copy-start.7 = (f32[192,2]{0,1:T(2,128)S(1)}, f32[192,2]{0,1:T(2,128)}, u32[]{:S(2)}) copy-start(f32[192,2]{0,1:T(2,128)} %param.18) | copy-start | bytes 4612
  7.2 157.5 %all-gather.4.cloned.1.call-start = ((), (), s32[]{:S(2)}) async-start(), calls=%async_computation.2 | async-start | bytes 18874368 | tf_op jit(solution)/shard_map/all_gather | solution.py:95
  10.5 236.0 %all-gather.6.cloned.1.call-start = ((), (), s32[]{:S(2)}) async-start(), calls=%async_computation.3 | async-start | bytes 9437184 | tf_op jit(solution)/shard_map/all_gather | solution.py:100
  18.0 20.4 %all-to-all-start = ((bf16[4,144,1024]{2,1,0:T(8,128)(2,1)}), bf16[4,144,1024]{2,1,0:T(8,128)(2,1)S(1)}, u32[]{:S(2)}, u32[]{:S(2)}) async-start(bf16[4,144,1024]{2,1,0:T(8,128)(2,1)} %bitcast.6), calls=%async_computation | async-start | bytes 2359296 | tf_op jit(solution)/shard_map/all_to_all | solution.py:92
  23.5 3.6 %collective-permute-start = (bf16[8,1024]{1,0:T(8,128)(2,1)S(1)}, bf16[8,1024]{1,0:T(8,128)(2,1)S(1)}, u32[]{:S(2)}, u32[]{:S(2)}) collective-permute-start(bf16[8,1024]{1,0:T(8,128)(2,1)S(1)} %get-tuple-element.7), channel_id=1, source_target_pairs={{0,1},{1,2},{2,3},{3,4},{4,5},{5,6},{6,7},{7,8},{8,9},{9,10},{10,1... | collective-permute-start | bytes 49160 | tf_op jit(solution)/shard_map/ppermute | solution.py:16
  25.0 4.7 %collective-permute-start.1 = (bf16[8,1024]{1,0:T(8,128)(2,1)S(1)}, bf16[8,1024]{1,0:T(8,128)(2,1)S(1)}, u32[]{:S(2)}, u32[]{:S(2)}) collective-permute-start(bf16[8,1024]{1,0:T(8,128)(2,1)S(1)} %get-tuple-element.8), channel_id=1, source_target_pairs={{1,0},{2,1},{3,2},{4,3},{5,4},{6,5},{7,6},{8,7},{9,8},{10,9},{11,1... | collective-permute-start | bytes 49160 | tf_op jit(solution)/shard_map/ppermute | solution.py:17
  164.8 11.7 %copy-start.8 = (bf16[2,1024,4096]{2,1,0:T(8,128)(2,1)S(1)}, bf16[2,1024,4096]{2,1,0:T(8,128)(2,1)}, u32[]{:S(2)}) copy-start(bf16[2,1024,4096]{2,1,0:T(8,128)(2,1)} %all-gather.4.cloned.1.call-done) | copy-start | bytes 50331652
  265.3 4.8 %copy-start.6 = (f32[1024]{0:T(1024)S(1)}, f32[1024]{0:T(1024)}, u32[]{:S(2)}) copy-start(f32[1024]{0:T(1024)} %param.14) | copy-start | bytes 12292
  265.3 19.4 %all-to-all-start.1 = ((bf16[4,144,1024]{2,1,0:T(8,128)(2,1)}), bf16[4,144,1024]{2,1,0:T(8,128)(2,1)S(1)}, u32[]{:S(2)}, u32[]{:S(2)}) async-start(bf16[4,144,1024]{2,1,0:T(8,128)(2,1)} %bitcast.54), calls=%async_computation.1 | async-start | bytes 2359296 | tf_op jit(solution)/shard_map/all_to_all | solution.py:112
Sparse Core Ops, SparseCore 0:
  10.6 154.1 all-gather.3
  166.4 80.0 all-gather.5
where the time goes:
time: 298 us
  waiting for transfers between devices  212 us (71%)
  matrix products  34.6 us (12%)
  other arithmetic  19.8 us (7%)
  between operations  14.3 us (5%)
  starting transfers between devices  12.1 us (4%)
  local copies, waits for them, and re-layouts  5.19 us (2%)
    all_gather x1, waiting for transfers between devices, on_device(): portion = lax.all_gather(paired, 'tp', axis=2, tiled=True)  126 us
    all_gather x1, waiting for transfers between devices, on_device(): portion = lax.all_gather(down_w, 'tp', axis=0, tiled=True)  59.9 us
    all_to_all x1, waiting for transfers between devices, on_device(): lax.all_to_all(result.astype(jnp.bfloat16), 'ep', split_axis=0, concat_ax...  13.7 us
    dot_general x1, matrix products, on_device(): jnp.einsum('rkf,kfd->krd', hidden_part, portion.reshape(blocks, block_wid...  11.5 us
    dot_general x1, matrix products, on_device(): up_part = jnp.dot(arrived, portion[1], preferred_element_type=jnp.float32)  11 us
    dot_general x1, matrix products, on_device(): gate_part = jnp.dot(arrived, portion[0], preferred_element_type=jnp.float32)  10.2 us
    all_to_all x1, waiting for transfers between devices, on_device(): lax.all_to_all(outgoing, 'ep', split_axis=0, concat_axis=0, tiled=True)  8.58 us
    reduce_sum x1, other arithmetic, on_device(): result = jnp.sum(rounded, axis=0)  7.32 us
  transfers between devices with their start and end apart: 6, of which 5 were waited for; matrix products, arithmetic and copies ran while one was open for 10% of the time, Pallas kernels for 0%

commit v1 on v0

--- a/solution.py
+++ b/solution.py
@@ -1,9 +1,14 @@
+import functools
+
 import jax
 import jax.numpy as jnp
 from jax import lax
+from jax.experimental import pallas as pl
+from jax.experimental.pallas import tpu as pltpu
 from jax.sharding import PartitionSpec as P
 
 epsilon = 1e-06
+vmem_share = 2**24
 
 
 def padded_2(value, sides, width):
@@ -49,19 +54,7 @@
     return jnp.stack(pooled_parts, axis=1).astype(jnp.bfloat16)
 
 
-def on_device(
-    mixer_input,
-    mixer_gain,
-    group_weight,
-    mixer_scale,
-    expert_input,
-    expert_gain,
-    routes,
-    route_weight,
-    w_gate,
-    w_up,
-    w_down,
-):
+def mixer(mixer_input, mixer_gain, group_weight, mixer_scale):
     row_count = mixer_input.shape[0]
     normed = normalize(mixer_input, mixer_gain)
     padded = padded_2(normed, ((("ep", "tp"), 0),), 8)
@@ -71,7 +64,10 @@
     mixed_groups = jnp.einsum(
         "tgi,gio->tgo", pooled, group_weight, preferred_element_type=jnp.float32
     )
-    mixer_out = (mixed_groups.reshape(row_count, -1) * mixer_scale).astype(jnp.bfloat16)
+    return (mixed_groups.reshape(row_count, -1) * mixer_scale).astype(jnp.bfloat16)
+
+
+def routed_plan(expert_input, expert_gain, routes, route_weight, w_gate, w_up, w_down):
     row_count = expert_input.shape[0]
     top_count = routes.shape[1]
     experts = lax.axis_size("ep") * w_gate.shape[0]
@@ -116,7 +112,336 @@
         jnp.take(returned, slot_index, axis=0).astype(jnp.float32).reshape(row_count, top_count, -1)
     )
     expert_out = jnp.sum(picked * route_weight[:, :, None], axis=1).astype(jnp.bfloat16)
-    return (mixer_out, expert_out)
+    return expert_out
+
+
+def slots(routes, route_weight, experts):
+    chosen = routes[:, :, None] == jnp.arange(experts, dtype=jnp.int32)[None, None, :]
+    named = jnp.any(chosen, axis=1)
+    weight = jnp.sum(jnp.where(chosen, route_weight[:, :, None], 0.0), axis=1)
+    rows = routes.shape[0]
+    earlier = jnp.arange(rows)[None, :] < jnp.arange(rows)[:, None]
+    place = jnp.dot(
+        earlier.astype(jnp.bfloat16), named.astype(jnp.bfloat16), preferred_element_type=jnp.float32
+    )
+    place = jnp.where(named, place, -1.0)
+    return jnp.stack([place.T, weight.T], axis=1)
+
+
+def near_first(length):
+    return [sorted(range(length), key=lambda other: abs(other - at)) for at in range(length)]
+
+
+def stream_kernel(
+    depth, capacity,
+    token_ref, listed_ref, gate_ref, up_ref, down_ref, out_ref,
+    tok, res, from_core, half_low, half_high, from_right, from_left, from_above, from_below,
+    send_sem, recv_sem, local_sem,
+):
+    column, line = lax.axis_index("ep"), lax.axis_index("tp")
+    level, core = line // 2, line % 2
+    other = 1 - core
+    rows = token_ref.shape[0]
+    half = rows // 2
+    right_column, left_column = (2 * column + 1) % 5, (3 * column + 2) % 5
+    right, left = (right_column, line), (left_column, line)
+    beside = (column, level * 2 + other)
+    above, below = (column, line + 2), (column, line - 2)
+    has_above, has_below = level < depth - 1, level > 0
+
+    def level_of(step):
+        value = 0
+        for at, order in enumerate(near_first(depth)):
+            for turn, there in enumerate(order):
+                value = value + there * jnp.where((level == at) & (step == turn), 1, 0)
+        return value
+
+    def link(src, dst, kind, at, target):
+        return pltpu.make_async_remote_copy(
+            src_ref=src, dst_ref=dst, send_sem=send_sem.at[kind, at],
+            recv_sem=recv_sem.at[kind, at], device_id=target,
+            device_id_type=pl.DeviceIdType.MESH,
+        )
+
+    def up(at):
+        return link(tok.at[at, 0, core], tok.at[at, 0, core], 0, at, above)
+
+    def down(at):
+        return link(tok.at[at, 0, core], tok.at[at, 0, core], 1, at, below)
+
+    def to_right(at):
+        return link(tok.at[at, 0, core], tok.at[at, 1, core], 2, at, right)
+
+    def to_left(at):
+        return link(tok.at[at, 0, core], tok.at[at, 2, core], 3, at, left)
+
+    def on_right(at):
+        part = pl.ds(0, half)
+        return link(tok.at[at, 1, core, part], tok.at[at, 3, core, part], 4, at, right)
+
+    def on_left(at):
+        part = pl.ds(half, half)
+        return link(tok.at[at, 2, core, part], tok.at[at, 3, core, part], 5, at, left)
+
+    def share(at, q):
+        return link(tok.at[at, q, core], tok.at[at, q, core], 6 + q, at, beside)
+
+    def shared_in(at, q):
+        return link(tok.at[at, q, other], tok.at[at, q, other], 6 + q, at, beside)
+
+    def give(at, q):
+        return link(res.at[at, q, other], from_core.at[at, q], 10 + q, at, beside)
+
+    def back_low(at):
+        return link(res.at[at, 3, core, pl.ds(0, half)], half_low.at[at], 14, at, left)
+
+    def back_high(at):
+        return link(res.at[at, 3, core, pl.ds(half, half)], half_high.at[at], 15, at, right)
+
+    def back_left(at):
+        return link(res.at[at, 1, core], from_right.at[at], 16, at, left)
+
+    def back_right(at):
+        return link(res.at[at, 2, core], from_left.at[at], 17, at, right)
+
+    def back_down(at):
+        return link(res.at[at, 0, core], from_above.at[at], 18, at, below)
+
+    def back_up(at):
+        return link(res.at[at, 0, core], from_below.at[at], 19, at, above)
+
+    barrier = pltpu.get_barrier_semaphore()
+
+    def greet(target):
+        pl.semaphore_signal(
+            barrier, inc=1, device_id=target, device_id_type=pl.DeviceIdType.MESH
+        )
+
+    greet(right)
+    greet(left)
+    greet(beside)
+    pl.when(has_above)(lambda: greet(above))
+    pl.when(has_below)(lambda: greet(below))
+    own_copy = pltpu.make_async_copy(token_ref, tok.at[level, 0, core], local_sem)
+    own_copy.start()
+    own_copy.wait()
+    pl.semaphore_wait(barrier, 3 + jnp.where(has_above, 1, 0) + jnp.where(has_below, 1, 0))
+
+    def compute(at, q):
+        source = (
+            jnp.where(q == 0, column, 0)
+            + jnp.where(q == 1, left_column, 0)
+            + jnp.where(q == 2, right_column, 0)
+            + jnp.where(q == 3, 3 - column, 0)
+        )
+        picks, scales, chosen = [], [], []
+        for lane in range(2):
+            listed = listed_ref[source * (2 * depth) + at * 2 + lane]
+            index = lax.broadcasted_iota(jnp.int32, (capacity, rows), 0).astype(jnp.float32)
+            hit = index == listed[0:1, :]
+            scales.append(jnp.sum(jnp.where(hit, listed[1:2, :], 0.0), axis=1, keepdims=True))
+            picks.append(jnp.where(hit, 1.0, 0.0).astype(jnp.bfloat16))
+            chosen.append(
+                jnp.dot(picks[lane], tok[at, q, lane], preferred_element_type=jnp.float32)
+                .astype(jnp.bfloat16)
+            )
+        gathered = jnp.concatenate(chosen, axis=0)
+        gate_part = jnp.dot(gathered, gate_ref[...], preferred_element_type=jnp.float32)
+        up_part = jnp.dot(gathered, up_ref[...], preferred_element_type=jnp.float32)
+        hidden = (gate_part / (1.0 + jnp.exp(-gate_part)) * up_part).astype(jnp.bfloat16)
+        partial = jnp.dot(hidden, down_ref[...], preferred_element_type=jnp.float32)
+        partial = (partial * jnp.concatenate(scales, axis=0)).astype(jnp.bfloat16)
+        for lane in range(2):
+            res[at, q, lane] = lax.dot_general(
+                picks[lane], partial[lane * capacity : (lane + 1) * capacity],
+                (((0,), (0,)), ((), ())), preferred_element_type=jnp.float32,
+            ).astype(jnp.bfloat16)
+
+    def stage(turn, carry):
+        @pl.when(turn < depth)
+        def _():
+            at = level_of(turn)
+            pl.when(at < level)(lambda: up(at).wait_recv())
+            pl.when(at > level)(lambda: down(at).wait_recv())
+            pl.when((at <= level) & has_above)(lambda: up(at).start())
+            pl.when((at >= level) & has_below)(lambda: down(at).start())
+            to_right(at).start()
+            to_left(at).start()
+            share(at, 0).start()
+
+        @pl.when((turn >= 1) & (turn < depth + 1))
+        def _():
+            at = level_of(turn - 1)
+            to_right(at).wait_recv()
+            on_right(at).start()
+            share(at, 1).start()
+            to_left(at).wait_recv()
+            on_left(at).start()
+            share(at, 2).start()
+
+        @pl.when(turn >= 2)
+        def _():
+            at = level_of(turn - 2)
+            on_right(at).wait_recv()
+            on_left(at).wait_recv()
+            share(at, 3).start()
+
+        def one(q, inner):
+            step = turn - (q + 1) // 2
+
+            @pl.when((step >= 0) & (step < depth))
+            def _():
+                at = level_of(step)
+                shared_in(at, q).wait_recv()
+                compute(at, q)
+                give(at, q).start()
+
+            return inner
+
+        lax.fori_loop(0, 4, one, 0)
+        return carry
+
+    lax.fori_loop(0, depth + 2, stage, 0)
+
+    piece = half // 3 if half % 48 == 0 else half
+    f32 = jnp.float32
+
+    def add(at, q, start, count, terms):
+        def body(i, carry):
+            span = pl.ds(pl.multiple_of(start + i * piece, piece), piece)
+            there = pl.ds(pl.multiple_of(i * piece, piece), piece)
+            total = res[at, q, core, span].astype(f32) + from_core[at, q, span].astype(f32)
+            for term in terms:
+                total = total + term[at, there].astype(f32)
+            res[at, q, core, span] = total.astype(jnp.bfloat16)
+            return carry
+
+        lax.fori_loop(0, count // piece, body, 0)
+
+    def extend(at, term):
+        def body(i, carry):
+            span = pl.ds(pl.multiple_of(i * piece, piece), piece)
+            res[at, 0, core, span] = (
+                res[at, 0, core, span].astype(f32) + term[at, span].astype(f32)
+            ).astype(jnp.bfloat16)
+            return carry
+
+        lax.fori_loop(0, rows // piece, body, 0)
+
+    def corner(turn, carry):
+        at = level_of(depth - 1 - turn)
+        give(at, 3).wait_recv()
+        add(at, 3, 0, rows, [])
+        back_low(at).start()
+        back_high(at).start()
+        return carry
+
+    def sides(at):
+        give(at, 1).wait_recv()
+        back_low(at).wait_recv()
+        add(at, 1, 0, half, [half_low])
+        add(at, 1, half, half, [])
+        back_left(at).start()
+        give(at, 2).wait_recv()
+        back_high(at).wait_recv()
+        add(at, 2, 0, half, [])
+        add(at, 2, half, half, [half_high])
+        back_right(at).start()
+
+    def home(at):
+        give(at, 0).wait_recv()
+        back_left(at).wait_recv()
+        back_right(at).wait_recv()
+        add(at, 0, 0, rows, [from_right, from_left])
+
+        @pl.when((at <= level) & has_above)
+        def _():
+            back_down(at).wait_recv()
+            extend(at, from_above)
+
+        @pl.when((at >= level) & has_below)
+        def _():
+            back_up(at).wait_recv()
+            extend(at, from_below)
+
+        pl.when(at < level)(lambda: back_down(at).start())
+        pl.when(at > level)(lambda: back_up(at).start())
+
+    def finish(turn, carry):
+        pl.when(turn < depth)(lambda: sides(level_of(depth - 1 - turn)))
+        pl.when(turn >= 1)(lambda: home(level_of(depth - turn)))
+        return carry
+
+    lax.fori_loop(0, depth, corner, 0)
+    lax.fori_loop(0, depth + 1, finish, 0)
+    out_copy = pltpu.make_async_copy(res.at[level, 0, core], out_ref, local_sem)
+    out_copy.start()
+
+    def drain(at, carry):
+        pl.when((at <= level) & has_above)(lambda: up(at).wait_send())
+        pl.when((at >= level) & has_below)(lambda: down(at).wait_send())
+        for copy in (to_right, to_left, on_right, on_left):
+            copy(at).wait_send()
+        for copy in (back_low, back_high, back_left, back_right):
+            copy(at).wait_send()
+        for q in range(4):
+            share(at, q).wait_send()
+            give(at, q).wait_send()
+        pl.when(at < level)(lambda: back_down(at).wait_send())
+        pl.when(at > level)(lambda: back_up(at).wait_send())
+        return carry
+
+    lax.fori_loop(0, depth, drain, 0)
+    out_copy.wait()
+
+
+def dense_plan(expert_input, expert_gain, routes, route_weight, w_gate, w_up, w_down):
+    row_count, width = expert_input.shape
+    experts = lax.axis_size("ep")
+    depth = lax.axis_size("tp") // 2
+    capacity = 3 * routes.shape[1] * row_count // (2 * experts)
+    axes = ("ep", "tp")
+    normed = normalize(expert_input, expert_gain)
+    listed = lax.all_gather(slots(routes, route_weight, experts), axes, axis=0)
+    mine = lax.dynamic_index_in_dim(listed, lax.axis_index("ep"), axis=1, keepdims=False)
+    bf16 = jnp.bfloat16
+    half = row_count // 2
+    vmem = pl.BlockSpec(memory_space=pltpu.VMEM)
+    return pl.pallas_call(
+        functools.partial(stream_kernel, depth, capacity),
+        out_shape=jax.ShapeDtypeStruct((row_count, width), bf16),
+        in_specs=[vmem] * 5,
+        out_specs=vmem,
+        scratch_shapes=[
+            pltpu.VMEM((depth, 4, 2, row_count, width), bf16),
+            pltpu.VMEM((depth, 4, 2, row_count, width), bf16),
+            pltpu.VMEM((depth, 4, row_count, width), bf16),
+            pltpu.VMEM((depth, half, width), bf16),
+            pltpu.VMEM((depth, half, width), bf16),
+            pltpu.VMEM((depth, row_count, width), bf16),
+            pltpu.VMEM((depth, row_count, width), bf16),
+            pltpu.VMEM((depth, row_count, width), bf16),
+            pltpu.VMEM((depth, row_count, width), bf16),
+            pltpu.SemaphoreType.DMA((20, depth)),
+            pltpu.SemaphoreType.DMA((20, depth)),
+            pltpu.SemaphoreType.DMA,
+        ],
+        compiler_params=pltpu.CompilerParams(
+            collective_id=0, has_side_effects=True, vmem_limit_bytes=60 * 2**20
+        ),
+    )(normed, mine, w_gate[0], w_up[0], w_down[0])
+
+
+def on_device(
+    mixer_input, mixer_gain, group_weight, mixer_scale,
+    expert_input, expert_gain, routes, route_weight, w_gate, w_up, w_down,
+):
+    devices = lax.axis_size(("ep", "tp"))
+    gathered_bytes = 2 * devices * expert_input.size
+    square = lax.axis_size("ep") == 4
+    plan = dense_plan if square and gathered_bytes <= vmem_share else routed_plan
+    expert_out = plan(expert_input, expert_gain, routes, route_weight, w_gate, w_up, w_down)
+    return (mixer(mixer_input, mixer_gain, group_weight, mixer_scale), expert_out)
 
 
 def solution(mesh):

time: 298 us -> 181 us (0.61)
  waiting for transfers between devices: 212 us -> 0.01 us
  Pallas kernels: 0 us -> 122 us
  blocking collectives: 0 us -> 46.2 us
  matrix products: 34.6 us -> 0.43 us
  other arithmetic: 19.8 us -> 4.64 us
  between operations: 14.3 us -> 0.83 us
  starting transfers between devices: 12.1 us -> 3.82 us
    all_gather x2 -> x0, waiting for transfers between devices: 186 us -> none  [the longest x1 126 us: on_device(): portion = lax.all_gather(paired, 'tp', axis=2, tiled=True)]
    pallas_call x0 -> x1, Pallas kernels: none -> 122 us  [dense_plan(): pl.pallas_call(functools.partial(stream_kernel, depth, capacity), out_sha...]
    all_gather x0 -> x1, blocking collectives: none -> 46.2 us  [dense_plan(): listed = lax.all_gather(slots(routes, route_weight, experts), axes, axis=0)]
    dot_general x5 -> x2, matrix products: 34.6 us -> 0.43 us  [the longest x1 0.28 us: mixer(): jnp.einsum('tgi,gio->tgo', pooled, group_weight, preferred_element_type=j...]
    all_to_all x2 -> x0, waiting for transfers between devices: 22.3 us -> none  [the longest x1 13.7 us: on_device(): lax.all_to_all(result.astype(jnp.bfloat16), 'ep', split_axis=0, concat_ax...]
    reduce_sum x3 -> x1, other arithmetic: 11.3 us -> 0.03 us  [slots(): weight = jnp.sum(jnp.where(chosen, route_weight[:, :, None], 0.0), axis=1)]
    all_to_all x2 -> x0, starting transfers between devices: 9.07 us -> none  [the longest x1 5.19 us: on_device(): lax.all_to_all(outgoing, 'ep', split_axis=0, concat_axis=0, tiled=True)]
    another operation x3 -> x1, other arithmetic: 4.57 us -> 0.01 us  [slots(): return jnp.stack([place.T, weight.T], axis=1)]
  transfers between devices with their start and end apart: 6 -> 2, of which waited for: 5 -> 0; matrix products, arithmetic and copies ran while one was open for 10% -> 1% of each run, Pallas kernels for 0% -> 68%
where the time goes in v1:
time: 181 us
  Pallas kernels  122 us (67%)
  blocking collectives  46.2 us (26%)
  other arithmetic  4.64 us (3%)
  starting transfers between devices  3.82 us (2%)
  local copies, waits for them, and re-layouts  2.4 us (1%)
    pallas_call x1, Pallas kernels, dense_plan(): pl.pallas_call(functools.partial(stream_kernel, depth, capacity), out_sha...  122 us
    all_gather x1, blocking collectives, dense_plan(): listed = lax.all_gather(slots(routes, route_weight, experts), axes, axis=0)  46.2 us
  transfers between devices with their start and end apart: 2, of which 0 were waited for; matrix products, arithmetic and copies ran while one was open for 1% of the time, Pallas kernels for 68%

profile of v1, /device:TPU:0, one launch (start us, length us, event | category | flops | bytes accessed | tf_op | source)
XLA Modules:
  0.0 180.6 jit_solution(16176898315729523418)
XLA Ops:
  0.6 0.0 copy-start
  0.6 0.0 copy-start.1
  0.7 1.2 fusion.1
  1.9 0.0 copy-done.1
  1.9 0.0 copy-start.4
  1.9 0.0 copy-start.7
  1.9 0.9 fusion.3
  2.8 0.0 copy-start.2
  2.8 2.5 %collective-permute-start = (bf16[8,1024]{1,0:T(8,128)(2,1)S(1)}, bf16[8,1024]{1,0:T(8,128)(2,1)S(1)}, u32[]{:S(2)}, u32[]{:S(2)}) collective-permute-start(bf16[8,1024]{1,0:T(8,128)(2,1)S(1)} %get-tuple-element.5), channel_id=1, source_target_pairs={{0,1},{1,2},{2,3},{3,4},{4,5},{5,6},{6,7},{7,8},{8,9},{9,10},{10,1... | collective-permute-start | bytes 49160 | tf_op jit(solution)/shard_map/ppermute | solution.py:21
  5.3 1.3 collective-permute-start.1
  6.7 0.0 copy-done.4
  6.7 0.1 fusion
  6.8 0.0 copy-done.7
  6.9 46.2 %all-gather = f32[128,2,192]{2,1,0:T(2,128)S(1)} all-gather(f32[4,2,192]{2,1,0:T(2,128)S(1)} %copy.25), channel_id=2, replica_groups=mesh['ep'=4,'tp'=8] {'ep','tp'}, dimensions={0}, use_global_device_ids=true | all-gather | bytes 202752 | tf_op jit(solution)/shard_map/all_gather | solution.py:405
  53.2 0.0 copy-done.2
  53.2 0.2 fusion.4
  53.3 0.0 copy-start.5
  53.3 0.7 dynamic-slice_bitcast_fusion.listed_ref
  54.0 0.0 copy-done.5
  54.0 0.9 fusion.6.token_ref
  54.9 122.3 %shard_map.122 = bf16[192,1024]{1,0:T(8,128)(2,1)} custom-call(bf16[192,1024]{1,0:T(8,128)(2,1)} %fusion.6.token_ref, f32[32,2,192]{2,1,0:T(2,128)} %dynamic-slice_bitcast_fusion.listed_ref, bf16[1024,512]{1,0:T(8,128)(2,1)} %bitcast.28, bf16[1024,512]{1,0:T(8,128)(2,1)} %bitcast.29, bf16[512,1024]{1,0:T(8,128)(2,1)} %bitcast.30), custom_call_target="tpu_custom_call" | custom-call | tf_op jit(solution)/shard_map/pallas_call | solution.py:410
  177.2 0.0 collective-permute-done
  177.2 0.0 collective-permute-done.1
  177.2 0.1 maximum_convert_fusion
  177.3 0.2 fusion.32
  177.5 0.3 fusion.29
  177.8 0.0 copy-done
  177.8 0.3 convolution_bitcast_fusion
  178.1 0.0 copy-start.6
  178.1 0.1 copy.26
  178.2 0.6 copy-done.6
  178.8 0.0 copy-start.3
  178.8 0.8 multiply_convert_fusion
  179.6 0.2 copy-done.3
  179.9 0.7 copy.28
  (9 shorter events, 0.1 us)
Async XLA Ops:
  0.6 177.2 %copy-start = (bf16[4,256,256]{2,1,0:T(8,128)(2,1)S(1)}, bf16[4,256,256]{2,1,0:T(8,128)(2,1)}, u32[]{:S(2)}) copy-start(bf16[4,256,256]{2,1,0:T(8,128)(2,1)} %param.13) | copy-start | bytes 1572868
  0.6 1.3 copy-start.1
  1.9 4.8 %copy-start.4 = (s32[192,2]{0,1:T(2,128)S(1)}, s32[192,2]{0,1:T(2,128)}, u32[]{:S(2)}) copy-start(s32[192,2]{0,1:T(2,128)} %param.17) | copy-start | bytes 4612
  1.9 4.9 %copy-start.7 = (f32[192,2]{0,1:T(2,128)S(1)}, f32[192,2]{0,1:T(2,128)}, u32[]{:S(2)}) copy-start(f32[192,2]{0,1:T(2,128)} %param.18) | copy-start | bytes 4612
  2.8 50.4 %copy-start.2 = (bf16[192,1024]{1,0:T(8,128)(2,1)S(1)}, bf16[192,1024]{1,0:T(8,128)(2,1)}, u32[]{:S(2)}) copy-start(bf16[192,1024]{1,0:T(8,128)(2,1)} %param.15) | copy-start | bytes 1179652
  2.8 174.4 %collective-permute-start = (bf16[8,1024]{1,0:T(8,128)(2,1)S(1)}, bf16[8,1024]{1,0:T(8,128)(2,1)S(1)}, u32[]{:S(2)}, u32[]{:S(2)}) collective-permute-start(bf16[8,1024]{1,0:T(8,128)(2,1)S(1)} %get-tuple-element.5), channel_id=1, source_target_pairs={{0,1},{1,2},{2,3},{3,4},{4,5},{5,6},{6,7},{7,8},{8,9},{9,10},{10,1... | collective-permute-start | bytes 49160 | tf_op jit(solution)/shard_map/ppermute | solution.py:21
  5.3 171.9 %collective-permute-start.1 = (bf16[8,1024]{1,0:T(8,128)(2,1)S(1)}, bf16[8,1024]{1,0:T(8,128)(2,1)S(1)}, u32[]{:S(2)}, u32[]{:S(2)}) collective-permute-start(bf16[8,1024]{1,0:T(8,128)(2,1)S(1)} %get-tuple-element.6), channel_id=1, source_target_pairs={{1,0},{2,1},{3,2},{4,3},{5,4},{6,5},{7,6},{8,7},{9,8},{10,9},{11,1... | collective-permute-start | bytes 49160 | tf_op jit(solution)/shard_map/ppermute | solution.py:22
  53.3 0.7 copy-start.5
  178.1 0.7 copy-start.6
  178.8 1.1 copy-start.3

commit v2 on v1

--- a/solution.py
+++ b/solution.py
@@ -125,7 +125,8 @@
         earlier.astype(jnp.bfloat16), named.astype(jnp.bfloat16), preferred_element_type=jnp.float32
     )
     place = jnp.where(named, place, -1.0)
-    return jnp.stack([place.T, weight.T], axis=1)
+    high = lax.reduce_precision(weight, 8, 7)
+    return jnp.concatenate([place, high, weight - high], axis=1).T.astype(jnp.bfloat16)
 
 
 def near_first(length):
@@ -133,15 +134,16 @@
 
 
 def stream_kernel(
-    depth, capacity,
-    token_ref, listed_ref, gate_ref, up_ref, down_ref, out_ref,
+    depth, capacity, experts,
+    token_ref, gate_ref, up_ref, down_ref, out_ref,
     tok, res, from_core, half_low, half_high, from_right, from_left, from_above, from_below,
     send_sem, recv_sem, local_sem,
 ):
     column, line = lax.axis_index("ep"), lax.axis_index("tp")
     level, core = line // 2, line % 2
     other = 1 - core
-    rows = token_ref.shape[0]
+    tall = token_ref.shape[0]
+    rows = out_ref.shape[0]
     half = rows // 2
     right_column, left_column = (2 * column + 1) % 5, (3 * column + 2) % 5
     right, left = (right_column, line), (left_column, line)
@@ -180,7 +182,7 @@
         return link(tok.at[at, 1, core, part], tok.at[at, 3, core, part], 4, at, right)
 
     def on_left(at):
-        part = pl.ds(half, half)
+        part = pl.ds(half, tall - half)
         return link(tok.at[at, 2, core, part], tok.at[at, 3, core, part], 5, at, left)
 
     def share(at, q):
@@ -227,22 +229,43 @@
     own_copy.wait()
     pl.semaphore_wait(barrier, 3 + jnp.where(has_above, 1, 0) + jnp.where(has_below, 1, 0))
 
+    piece = half // 3 if half % 48 == 0 else half
+    f32 = jnp.float32
+
+    def add(at, q, start, count, terms):
+        def body(i, carry):
+            span = pl.ds(pl.multiple_of(start + i * piece, piece), piece)
+            there = pl.ds(pl.multiple_of(i * piece, piece), piece)
+            total = res[at, q, core, span].astype(f32) + from_core[at, q, span].astype(f32)
+            for term in terms:
+                total = total + term[at, there].astype(f32)
+            res[at, q, core, span] = total.astype(jnp.bfloat16)
+            return carry
+
+        lax.fori_loop(0, count // piece, body, 0)
+
+    def corner(at):
+        give(at, 3).wait_recv()
+        add(at, 3, 0, rows, [])
+        back_low(at).start()
+        back_high(at).start()
+
     def compute(at, q):
-        source = (
-            jnp.where(q == 0, column, 0)
-            + jnp.where(q == 1, left_column, 0)
-            + jnp.where(q == 2, right_column, 0)
-            + jnp.where(q == 3, 3 - column, 0)
-        )
         picks, scales, chosen = [], [], []
         for lane in range(2):
-            listed = listed_ref[source * (2 * depth) + at * 2 + lane]
+            listed = tok[at, q, lane, pl.ds(rows, tall - rows), pl.ds(0, rows)].astype(f32)
+            listing = lax.broadcasted_iota(jnp.int32, listed.shape, 0)
+
+            def row_of(index):
+                return jnp.sum(jnp.where(listing == index, listed, 0.0), axis=0, keepdims=True)
+
+            weight = row_of(experts + column) + row_of(2 * experts + column)
             index = lax.broadcasted_iota(jnp.int32, (capacity, rows), 0).astype(jnp.float32)
-            hit = index == listed[0:1, :]
-            scales.append(jnp.sum(jnp.where(hit, listed[1:2, :], 0.0), axis=1, keepdims=True))
+            hit = index == row_of(column)
+            scales.append(jnp.sum(jnp.where(hit, weight, 0.0), axis=1, keepdims=True))
             picks.append(jnp.where(hit, 1.0, 0.0).astype(jnp.bfloat16))
             chosen.append(
-                jnp.dot(picks[lane], tok[at, q, lane], preferred_element_type=jnp.float32)
+                jnp.dot(picks[lane], tok[at, q, lane, pl.ds(0, rows)], preferred_element_type=jnp.float32)
                 .astype(jnp.bfloat16)
             )
         gathered = jnp.concatenate(chosen, axis=0)
@@ -279,12 +302,14 @@
             on_left(at).start()
             share(at, 2).start()
 
-        @pl.when(turn >= 2)
+        @pl.when((turn >= 2) & (turn < depth + 2))
         def _():
             at = level_of(turn - 2)
             on_right(at).wait_recv()
             on_left(at).wait_recv()
             share(at, 3).start()
+
+        pl.when(turn >= 3)(lambda: corner(level_of(turn - 3)))
 
         def one(q, inner):
             step = turn - (q + 1) // 2
@@ -301,22 +326,7 @@
         lax.fori_loop(0, 4, one, 0)
         return carry
 
-    lax.fori_loop(0, depth + 2, stage, 0)
-
-    piece = half // 3 if half % 48 == 0 else half
-    f32 = jnp.float32
-
-    def add(at, q, start, count, terms):
-        def body(i, carry):
-            span = pl.ds(pl.multiple_of(start + i * piece, piece), piece)
-            there = pl.ds(pl.multiple_of(i * piece, piece), piece)
-            total = res[at, q, core, span].astype(f32) + from_core[at, q, span].astype(f32)
-            for term in terms:
-                total = total + term[at, there].astype(f32)
-            res[at, q, core, span] = total.astype(jnp.bfloat16)
-            return carry
-
-        lax.fori_loop(0, count // piece, body, 0)
+    lax.fori_loop(0, depth + 3, stage, 0)
 
     def extend(at, term):
         def body(i, carry):
@@ -327,14 +337,6 @@
             return carry
 
         lax.fori_loop(0, rows // piece, body, 0)
-
-    def corner(turn, carry):
-        at = level_of(depth - 1 - turn)
-        give(at, 3).wait_recv()
-        add(at, 3, 0, rows, [])
-        back_low(at).start()
-        back_high(at).start()
-        return carry
 
     def sides(at):
         give(at, 1).wait_recv()
@@ -372,7 +374,6 @@
         pl.when(turn >= 1)(lambda: home(level_of(depth - turn)))
         return carry
 
-    lax.fori_loop(0, depth, corner, 0)
     lax.fori_loop(0, depth + 1, finish, 0)
     out_copy = pltpu.make_async_copy(res.at[level, 0, core], out_ref, local_sem)
     out_copy.start()
@@ -400,20 +401,21 @@
     experts = lax.axis_size("ep")
     depth = lax.axis_size("tp") // 2
     capacity = 3 * routes.shape[1] * row_count // (2 * experts)
-    axes = ("ep", "tp")
     normed = normalize(expert_input, expert_gain)
-    listed = lax.all_gather(slots(routes, route_weight, experts), axes, axis=0)
-    mine = lax.dynamic_index_in_dim(listed, lax.axis_index("ep"), axis=1, keepdims=False)
+    listed = slots(routes, route_weight, experts)
+    pad = -(-3 * experts // 16) * 16
+    listed = jnp.pad(listed, ((0, pad - 3 * experts), (0, width - row_count)))
+    sent = jnp.concatenate([normed, listed], axis=0)
     bf16 = jnp.bfloat16
     half = row_count // 2
     vmem = pl.BlockSpec(memory_space=pltpu.VMEM)
     return pl.pallas_call(
-        functools.partial(stream_kernel, depth, capacity),
+        functools.partial(stream_kernel, depth, capacity, experts),
         out_shape=jax.ShapeDtypeStruct((row_count, width), bf16),
-        in_specs=[vmem] * 5,
+        in_specs=[vmem] * 4,
         out_specs=vmem,
         scratch_shapes=[
-            pltpu.VMEM((depth, 4, 2, row_count, width), bf16),
+            pltpu.VMEM((depth, 4, 2, row_count + pad, width), bf16),
             pltpu.VMEM((depth, 4, 2, row_count, width), bf16),
             pltpu.VMEM((depth, 4, row_count, width), bf16),
             pltpu.VMEM((depth, half, width), bf16),
@@ -429,7 +431,7 @@
         compiler_params=pltpu.CompilerParams(
             collective_id=0, has_side_effects=True, vmem_limit_bytes=60 * 2**20
         ),
-    )(normed, mine, w_gate[0], w_up[0], w_down[0])
+    )(sent, w_gate[0], w_up[0], w_down[0])
 
 
 def on_device(

time: 181 us -> 143 us (0.79)
  blocking collectives: 46.2 us -> 0 us
  Pallas kernels: 122 us -> 130 us
    all_gather x1 -> x0, blocking collectives: 46.2 us -> none  [dense_plan(): listed = lax.all_gather(slots(routes, route_weight, experts), axes, axis=0)]
    pallas_call x1, Pallas kernels: 122 us -> 130 us  [dense_plan(): pl.pallas_call(functools.partial(stream_kernel, depth, capacity, experts)...]
  transfers between devices with their start and end apart: 2 -> 2, of which waited for: 0 -> 0; matrix products, arithmetic and copies ran while one was open for 1% -> 1% of each run, Pallas kernels for 68% -> 91%
where the time goes in v2:
time: 143 us
  Pallas kernels  130 us (91%)
  other arithmetic  4.74 us (3%)
  starting transfers between devices  3.69 us (3%)
  local copies, waits for them, and re-layouts  3.54 us (2%)
    pallas_call x1, Pallas kernels, dense_plan(): pl.pallas_call(functools.partial(stream_kernel, depth, capacity, experts)...  130 us
    unnamed x17, local copies, waits for them, and re-layouts  3.46 us
  transfers between devices with their start and end apart: 2, of which 0 were waited for; matrix products, arithmetic and copies ran while one was open for 1% of the time, Pallas kernels for 91%

profile of v2, /device:TPU:0, one launch (start us, length us, event | category | flops | bytes accessed | tf_op | source)
XLA Modules:
  0.0 143.1 jit_solution(18363904212054140669)
XLA Ops:
  0.6 0.0 copy-start
  0.6 0.0 copy-start.1
  0.7 1.2 fusion.2
  1.9 0.0 copy-done.1
  1.9 0.0 copy-start.2
  1.9 0.9 fusion.4
  2.8 2.4 %collective-permute-start = (bf16[8,1024]{1,0:T(8,128)(2,1)S(1)}, bf16[8,1024]{1,0:T(8,128)(2,1)S(1)}, u32[]{:S(2)}, u32[]{:S(2)}) collective-permute-start(bf16[8,1024]{1,0:T(8,128)(2,1)S(1)} %get-tuple-element.5), channel_id=1, source_target_pairs={{0,1},{1,2},{2,3},{3,4},{4,5},{5,6},{6,7},{7,8},{8,9},{9,10},{10,1... | collective-permute-start | bytes 49160 | tf_op jit(solution)/shard_map/ppermute | solution.py:21
  5.2 1.3 collective-permute-start.1
  6.5 0.0 copy-start.4
  6.6 0.7 copy-done.4
  7.2 0.0 copy-start.7
  7.2 0.7 copy-done.7
  7.9 0.1 fusion
  8.1 0.0 copy-done.2
  8.1 0.0 copy-start.5
  8.1 0.2 fusion.5
  8.3 0.5 copy-done.5
  8.8 0.2 fusion.7
  9.0 0.8 fusion.8.token_ref
  9.8 129.9 %shard_map.122 = bf16[192,1024]{1,0:T(8,128)(2,1)} custom-call(bf16[208,1024]{1,0:T(8,128)(2,1)} %fusion.8.token_ref, bf16[1024,512]{1,0:T(8,128)(2,1)} %bitcast.20, bf16[1024,512]{1,0:T(8,128)(2,1)} %bitcast.21, bf16[512,1024]{1,0:T(8,128)(2,1)} %bitcast.22), custom_call_target="tpu_custom_call" | custom-call | tf_op jit(solution)/shard_map/pallas_call | solution.py:412
  139.7 0.0 collective-permute-done
  139.7 0.0 collective-permute-done.1
  139.7 0.1 maximum_convert_fusion
  139.8 0.2 fusion.34
  140.0 0.3 fusion.31
  140.3 0.0 copy-done
  140.3 0.3 convolution_bitcast_fusion
  140.6 0.0 copy-start.6
  140.6 0.1 copy.19
  140.7 0.6 copy-done.6
  141.3 0.0 copy-start.3
  141.3 0.8 multiply_convert_fusion
  142.1 0.2 copy-done.3
  142.4 0.7 copy.21
  (9 shorter events, 0.1 us)
Async XLA Ops:
  0.6 139.7 %copy-start = (bf16[4,256,256]{2,1,0:T(8,128)(2,1)S(1)}, bf16[4,256,256]{2,1,0:T(8,128)(2,1)}, u32[]{:S(2)}) copy-start(bf16[4,256,256]{2,1,0:T(8,128)(2,1)} %param.13) | copy-start | bytes 1572868
  0.6 1.3 copy-start.1
  1.9 6.2 %copy-start.2 = (bf16[192,1024]{1,0:T(8,128)(2,1)S(1)}, bf16[192,1024]{1,0:T(8,128)(2,1)}, u32[]{:S(2)}) copy-start(bf16[192,1024]{1,0:T(8,128)(2,1)} %param.15) | copy-start | bytes 1179652
  2.8 136.8 %collective-permute-start = (bf16[8,1024]{1,0:T(8,128)(2,1)S(1)}, bf16[8,1024]{1,0:T(8,128)(2,1)S(1)}, u32[]{:S(2)}, u32[]{:S(2)}) collective-permute-start(bf16[8,1024]{1,0:T(8,128)(2,1)S(1)} %get-tuple-element.5), channel_id=1, source_target_pairs={{0,1},{1,2},{2,3},{3,4},{4,5},{5,6},{6,7},{7,8},{8,9},{9,10},{10,1... | collective-permute-start | bytes 49160 | tf_op jit(solution)/shard_map/ppermute | solution.py:21
  5.2 134.5 %collective-permute-start.1 = (bf16[8,1024]{1,0:T(8,128)(2,1)S(1)}, bf16[8,1024]{1,0:T(8,128)(2,1)S(1)}, u32[]{:S(2)}, u32[]{:S(2)}) collective-permute-start(bf16[8,1024]{1,0:T(8,128)(2,1)S(1)} %get-tuple-element.6), channel_id=1, source_target_pairs={{1,0},{2,1},{3,2},{4,3},{5,4},{6,5},{7,6},{8,7},{9,8},{10,9},{11,1... | collective-permute-start | bytes 49160 | tf_op jit(solution)/shard_map/ppermute | solution.py:22
  6.5 0.7 copy-start.4
  7.2 0.7 copy-start.7
  8.1 0.7 copy-start.5
  140.6 0.7 copy-start.6
  141.3 1.1 copy-start.3

commit v3 on v2

--- a/solution.py
+++ b/solution.py
@@ -370,10 +370,11 @@
         pl.when(at > level)(lambda: back_up(at).start())
 
     def finish(turn, carry):
-        pl.when(turn < depth)(lambda: sides(level_of(depth - 1 - turn)))
+        pl.when(turn < depth - 1)(lambda: sides(level_of(depth - 1 - turn)))
         pl.when(turn >= 1)(lambda: home(level_of(depth - turn)))
         return carry
 
+    sides(level)
     lax.fori_loop(0, depth + 1, finish, 0)
     out_copy = pltpu.make_async_copy(res.at[level, 0, core], out_ref, local_sem)
     out_copy.start()

time: 143 us -> 151 us (1.056); the launches traced: 143 us -> 149 us
  Pallas kernels: 130 us -> 136 us
    pallas_call x1, Pallas kernels: 130 us -> 136 us  [dense_plan(): pl.pallas_call(functools.partial(stream_kernel, depth, capacity, experts)...]
where the time goes in v3:
time: 151 us; the launch traced here: 149 us
  Pallas kernels  136 us (90%)
  other arithmetic  4.74 us (3%)
  starting transfers between devices  3.69 us (2%)
  local copies, waits for them, and re-layouts  3.54 us (2%)
    pallas_call x1, Pallas kernels, dense_plan(): pl.pallas_call(functools.partial(stream_kernel, depth, capacity, experts)...  136 us
    unnamed x17, local copies, waits for them, and re-layouts  3.46 us
  transfers between devices with their start and end apart: 2, of which 0 were waited for; matrix products, arithmetic and copies ran while one was open for 1% of the time, Pallas kernels for 91%

profile of v3, /device:TPU:0, one launch (start us, length us, event | category | flops | bytes accessed | tf_op | source)
XLA Modules:
  0.0 149.5 jit_solution(3177526504917815575)
XLA Ops:
  0.6 0.0 copy-start
  0.6 0.0 copy-start.1
  0.7 1.2 fusion.2
  1.9 0.0 copy-done.1
  1.9 0.0 copy-start.2
  1.9 0.9 fusion.4
  2.8 2.4 %collective-permute-start = (bf16[8,1024]{1,0:T(8,128)(2,1)S(1)}, bf16[8,1024]{1,0:T(8,128)(2,1)S(1)}, u32[]{:S(2)}, u32[]{:S(2)}) collective-permute-start(bf16[8,1024]{1,0:T(8,128)(2,1)S(1)} %get-tuple-element.5), channel_id=1, source_target_pairs={{0,1},{1,2},{2,3},{3,4},{4,5},{5,6},{6,7},{7,8},{8,9},{9,10},{10,1... | collective-permute-start | bytes 49160 | tf_op jit(solution)/shard_map/ppermute | solution.py:21
  5.2 1.3 collective-permute-start.1
  6.5 0.0 copy-start.4
  6.6 0.7 copy-done.4
  7.2 0.0 copy-start.7
  7.2 0.7 copy-done.7
  7.9 0.1 fusion
  8.1 0.0 copy-done.2
  8.1 0.0 copy-start.5
  8.1 0.2 fusion.5
  8.3 0.5 copy-done.5
  8.8 0.2 fusion.7
  9.0 0.8 fusion.8.token_ref
  9.8 136.3 %shard_map.122 = bf16[192,1024]{1,0:T(8,128)(2,1)} custom-call(bf16[208,1024]{1,0:T(8,128)(2,1)} %fusion.8.token_ref, bf16[1024,512]{1,0:T(8,128)(2,1)} %bitcast.20, bf16[1024,512]{1,0:T(8,128)(2,1)} %bitcast.21, bf16[512,1024]{1,0:T(8,128)(2,1)} %bitcast.22), custom_call_target="tpu_custom_call" | custom-call | tf_op jit(solution)/shard_map/pallas_call | solution.py:413
  146.0 0.0 collective-permute-done
  146.0 0.0 collective-permute-done.1
  146.1 0.1 maximum_convert_fusion
  146.1 0.2 fusion.34
  146.4 0.3 fusion.31
  146.7 0.0 copy-done
  146.7 0.3 convolution_bitcast_fusion
  147.0 0.0 copy-start.6
  147.0 0.1 copy.19
  147.1 0.6 copy-done.6
  147.6 0.0 copy-start.3
  147.6 0.8 multiply_convert_fusion
  148.5 0.2 copy-done.3
  148.7 0.7 copy.21
  (9 shorter events, 0.1 us)
Async XLA Ops:
  0.6 146.0 %copy-start = (bf16[4,256,256]{2,1,0:T(8,128)(2,1)S(1)}, bf16[4,256,256]{2,1,0:T(8,128)(2,1)}, u32[]{:S(2)}) copy-start(bf16[4,256,256]{2,1,0:T(8,128)(2,1)} %param.13) | copy-start | bytes 1572868
  0.6 1.3 copy-start.1
  1.9 6.2 %copy-start.2 = (bf16[192,1024]{1,0:T(8,128)(2,1)S(1)}, bf16[192,1024]{1,0:T(8,128)(2,1)}, u32[]{:S(2)}) copy-start(bf16[192,1024]{1,0:T(8,128)(2,1)} %param.15) | copy-start | bytes 1179652
  2.8 143.2 %collective-permute-start = (bf16[8,1024]{1,0:T(8,128)(2,1)S(1)}, bf16[8,1024]{1,0:T(8,128)(2,1)S(1)}, u32[]{:S(2)}, u32[]{:S(2)}) collective-permute-start(bf16[8,1024]{1,0:T(8,128)(2,1)S(1)} %get-tuple-element.5), channel_id=1, source_target_pairs={{0,1},{1,2},{2,3},{3,4},{4,5},{5,6},{6,7},{7,8},{8,9},{9,10},{10,1... | collective-permute-start | bytes 49160 | tf_op jit(solution)/shard_map/ppermute | solution.py:21
  5.2 140.8 %collective-permute-start.1 = (bf16[8,1024]{1,0:T(8,128)(2,1)S(1)}, bf16[8,1024]{1,0:T(8,128)(2,1)S(1)}, u32[]{:S(2)}, u32[]{:S(2)}) collective-permute-start(bf16[8,1024]{1,0:T(8,128)(2,1)S(1)} %get-tuple-element.6), channel_id=1, source_target_pairs={{1,0},{2,1},{3,2},{4,3},{5,4},{6,5},{7,6},{8,7},{9,8},{10,9},{11,1... | collective-permute-start | bytes 49160 | tf_op jit(solution)/shard_map/ppermute | solution.py:22
  6.5 0.7 copy-start.4
  7.2 0.7 copy-start.7
  8.1 0.7 copy-start.5
  147.0 0.7 copy-start.6
  147.6 1.1 copy-start.3
